TPU v7x, 32 devices: a whole 2x2x4 slice. The times are simulated.
32 devices in a mesh: ep: 4 (over y, x), tp: 8 (over z, core).
Axes of the slice: x: 2, y: 2, z: 4, core: 2. Of those that a mesh axis runs over, the one named last changes fastest.
Arguments:
- stream: bfloat16 [16384, 1024], P(('ep', 'tp')), may hold values from -6 to 6
- norm_gain: float32 [1024], replicated, may hold values from 0.5 to 1.5
- gate_rows: bfloat16 [4, 1024, 1024], P('ep', 'tp'), may hold values from -0.1875 to 0.1875
- up_rows: bfloat16 [4, 1024, 1024], P('ep', 'tp'), may hold values from -0.1875 to 0.1875
- down_rows: bfloat16 [4, 1024, 1024], P('ep', 'tp'), may hold values from -0.1875 to 0.1875
- chosen: int32 [4, 8192], P('ep'), may hold values from 0 to 16383, as said below
- affinity: float32 [4, 8192], P('ep'), may hold values from 0.2 to 1
Outputs:
- mixed_out: bfloat16 [16384, 1024], P(('ep', 'tp'))
Inputs may be any that keep to these rules, and one draw needn't show every extreme that they name: Each row of chosen names 8192 different token numbers in increasing order. Among the 512 consecutive token numbers of any one device, an expert reads at most 512, and for every expert some device holds exactly 512 of its tokens.
All inputs are finite; a program needn't handle non-finite values.
Results may differ from a plain program's by a relative error of at most 0.008.
Values may be sent and summed in bfloat16 or wider, within the bound.
A program may use at most 64 MiB of HBM per device.

v0:
```python
import jax
import jax.numpy as jnp
from jax import lax
from jax.sharding import PartitionSpec as P

epsilon = 1e-06


def over_all(piece, axis, dim, step, start):
    def gathered(part):
        return lax.all_gather(part, axis, axis=dim, tiled=True)

    return step(start, jax.tree.map(gathered, piece), jnp.int32(0))


def shortened(array):
    def short(part):
        return part.astype(jnp.bfloat16) if part.dtype == jnp.float32 else part

    return jax.tree.map(short, array)


def normalize(stream, norm_gain):
    values = stream.astype(jnp.float32)
    inverse = lax.rsqrt(jnp.mean(values * values, axis=-1, keepdims=True) + epsilon)
    return (values * inverse * norm_gain).astype(jnp.bfloat16)


def cut_slices(padded, starts, length):
    return jax.vmap(lambda offset: lax.dynamic_slice_in_dim(padded, offset, length))(starts)


def own_slice(listed, padded, boundary, length):
    offset = jnp.searchsorted(listed, boundary).astype(jnp.int32)
    return lax.dynamic_slice_in_dim(padded, offset, length)


def add_slice(inputs, running, pieces):
    gate_piece, up_piece, down_piece = pieces
    gate_sum = jnp.einsum("erd,efd->erf", inputs, gate_piece, preferred_element_type=jnp.float32)
    up_sum = jnp.einsum("erd,efd->erf", inputs, up_piece, preferred_element_type=jnp.float32)
    hidden = (jax.nn.silu(gate_sum) * up_sum).astype(jnp.bfloat16)
    return running + jnp.einsum(
        "erf,efd->erd", hidden, down_piece, preferred_element_type=jnp.float32
    )


def per_device(stream, norm_gain, gate_rows, up_rows, down_rows, chosen, affinity):
    ep_count = lax.axis_size("ep")
    tp_count = lax.axis_size("tp")
    row_count, feature_count = stream.shape
    local_experts = chosen.shape[0]
    slot_count = 4 * row_count // (local_experts * ep_count)
    tp_index = lax.axis_index("tp")
    first_token = (lax.axis_index("ep") * tp_count + tp_index) * row_count
    weight_sets = (gate_rows, up_rows, down_rows)
    normed = normalize(stream, norm_gain)
    column_bounds = (jnp.arange(ep_count, dtype=jnp.int32) * tp_count + tp_index) * row_count
    column_starts = jax.vmap(
        lambda listed: jnp.searchsorted(listed, column_bounds).astype(jnp.int32)
    )(chosen)
    padded_weights = jnp.concatenate(
        [affinity, jnp.zeros((local_experts, slot_count), jnp.float32)], axis=1
    )
    slot_weights = jax.vmap(lambda padded, starts: cut_slices(padded, starts, slot_count))(
        padded_weights, column_starts
    )
    slot_weights = jnp.transpose(slot_weights, (1, 0, 2))
    all_lists = lax.all_gather(chosen, "ep", axis=0, tiled=True)
    padded_all = jnp.concatenate(
        [all_lists, jnp.full((all_lists.shape[0], slot_count), -1, jnp.int32)], axis=1
    )
    own_picks = jax.vmap(lambda listed, padded: own_slice(listed, padded, first_token, slot_count))(
        all_lists, padded_all
    )
    own_picks = own_picks.reshape(ep_count, local_experts, slot_count)
    local_rows = own_picks - first_token
    usable = (local_rows >= 0) & (local_rows < row_count)
    safe_rows = jnp.where(usable, local_rows, 0)
    outgoing = jnp.take(normed, safe_rows.reshape(-1), axis=0)
    outgoing = outgoing.reshape(ep_count, local_experts, slot_count, feature_count)
    outgoing = jnp.where(usable[..., None], outgoing, jnp.zeros((), jnp.bfloat16))
    arrived = lax.all_to_all(outgoing, "ep", split_axis=0, concat_axis=0, tiled=True)
    inputs = jnp.transpose(arrived, (1, 0, 2, 3)).reshape(
        local_experts, ep_count * slot_count, feature_count
    )
    initial = jnp.zeros((local_experts, ep_count * slot_count, feature_count), jnp.float32)
    produced = over_all(
        (weight_sets[0], weight_sets[1], weight_sets[2]),
        "tp",
        1,
        lambda running, pieces, anchor: add_slice(inputs, running, pieces),
        initial,
    )
    produced = produced.astype(jnp.bfloat16).reshape(
        local_experts, ep_count, slot_count, feature_count
    )
    produced = jnp.transpose(produced, (1, 0, 2, 3))
    produced = lax.optimization_barrier(produced)
    weighted = produced.astype(jnp.float32) * slot_weights[..., None]
    returned = lax.all_to_all(
        shortened(weighted), "ep", split_axis=0, concat_axis=0, tiled=True
    ).astype(weighted.dtype)
    segment_ids = jnp.where(usable, local_rows, row_count).reshape(-1)
    summed = jax.ops.segment_sum(
        returned.reshape(-1, feature_count), segment_ids, num_segments=row_count + 1
    )
    return summed[:row_count].astype(jnp.bfloat16)


def solution(mesh):
    return jax.shard_map(
        per_device,
        mesh=mesh,
        in_specs=(
            P(("ep", "tp"), None),
            P(),
            P("ep", "tp", None),
            P("ep", "tp", None),
            P("ep", "tp", None),
            P("ep", None),
            P("ep", None),
        ),
        out_specs=P(("ep", "tp"), None),
        check_vma=False,
    )
```

profile of v0, /device:TPU:0, one launch (start us, length us, event | category | flops | bytes accessed | tf_op | source)
XLA Modules:
  0.0 207.0 jit_solution(7549158890057744345)
XLA Ops:
  6.5 0.7 all-gather.5.cloned.1.call-update
  7.3 0.7 all-gather.9.cloned.1.call-update
  8.0 10.2 %all-gather = s32[4,1,8192]{2,1,0:T(1,128)S(1)} all-gather(s32[1,1,8192]{2,1,0:T(1,128)} %bitcast.83), channel_id=1, replica_groups=mesh['ep'=4,'tp'=8] {'ep'}, dimensions={0}, use_global_device_ids=true | all-gather | bytes 163840 | tf_op jit(solution)/shard_map/all_gather | solution.py:69
  18.3 9.6 %while.53 = (s32[]{:T(128)}, u32[4]{0:T(128)S(1)}, u32[4]{0:T(128)S(1)}, s32[]{:T(128)}, s32[4,8192]{1,0:T(4,128)S(1)}) while((s32[]{:T(128)}, u32[4]{0:T(128)S(1)}, u32[4]{0:T(128)S(1)}, s32[]{:T(128)}, s32[4,8192]{1,0:T(4,128)S(1)}) %tuple.122), condition=%wide.region_1.2_spmd.clone.clone, body=%wide.region_0.0_spmd.clone.sunk.clone | while | flops 75 | bytes 276 | solution.py:34
  18.3 0.6 gather_fusion
  19.0 0.6 gather_fusion
  19.7 0.6 gather_fusion
  20.4 0.6 gather_fusion
  21.1 0.6 gather_fusion
  21.8 0.6 gather_fusion
  22.5 0.6 gather_fusion
  23.2 0.6 gather_fusion
  23.8 0.6 gather_fusion
  24.5 0.6 gather_fusion
  25.2 0.6 gather_fusion
  25.9 0.6 gather_fusion
  26.6 0.6 gather_fusion
  27.3 0.6 gather_fusion
  28.0 8.5 %while.51 = (s32[]{:T(128)}, s32[4,8704]{1,0:T(4,128)S(1)}, s32[4,2]{0,1:T(2,128)S(1)}, s32[4,512]{1,0:T(4,128)S(1)}) while((s32[]{:T(128)}, s32[4,8704]{1,0:T(4,128)S(1)}, s32[4,2]{0,1:T(2,128)S(1)}, s32[4,512]{1,0:T(4,128)S(1)}) %tuple.106), condition=%wide.while_cond.clone, body=%wide.while_body.sunk.clone | while | flops 2 | bytes 8297 | solution.py:35
  28.7 1.4 dynamic-slice.19
  30.8 1.4 dynamic-slice.19
  33.0 1.4 dynamic-slice.19
  35.1 1.4 dynamic-slice.19
  37.2 9.7 %gather_fusion.2 = bf16[2048,1024]{1,0:T(8,128)(2,1)} fusion(bf16[512,1024]{1,0:T(8,128)(2,1)S(1)} %fusion.8, s32[2048]{0:T(1024)S(1)} %broadcast_clamp_fusion), kind=kCustom, calls=%fused_computation.2 | custom fusion | bytes 8396800 | tf_op jit(solution)/shard_map/jit(_take)/gather | solution.py:80
  47.0 3.9 %select_select_fusion = bf16[4,1,512,1024]{3,2,1,0:T(8,128)(2,1)} fusion(bf16[4,1,512,1024]{3,2,1,0:T(8,128)(2,1)} %bitcast.85, pred[4,512]{1,0:T(4,128)(4,1)S(1)} %get-tuple-element.235, pred[4,512]{1,0:T(4,128)(4,1)S(1)} %get-tuple-element.234), kind=kLoop, calls=%fused_computation.28 | loop fusion | flops 4194304 | bytes 8392704 | tf_op jit(solution)/shard_map/jit(_where)/select_n | solution.py:82
  50.9 5.0 %all-to-all-start = ((bf16[4,1,512,1024]{3,2,1,0:T(8,128)(2,1)}), bf16[4,1,512,1024]{3,2,1,0:T(8,128)(2,1)}, u32[]{:S(2)}, u32[]{:S(2)}) async-start(bf16[4,1,512,1024]{3,2,1,0:T(8,128)(2,1)} %select_select_fusion), calls=%async_computation | async-start | bytes 8388608 | tf_op jit(solution)/shard_map/all_to_all | solution.py:83
  56.0 0.7 all-gather.7.cloned.1.call-update
  56.7 10.0 %while.54 = (s32[]{:T(128)}, u32[1,4]{1,0:T(1,128)S(1)}, u32[1,4]{1,0:T(1,128)S(1)}, s32[1,8192]{1,0:T(1,128)S(1)}, s32[]{:T(128)}) while((s32[]{:T(128)}, u32[1,4]{1,0:T(1,128)S(1)}, u32[1,4]{1,0:T(1,128)S(1)}, s32[1,8192]{1,0:T(1,128)S(1)}, s32[]{:T(128)}) %tuple.121), condition=%wide.region_4.5_spmd.clone.clone, body=%wide.region_3.4_spmd.clone.sunk.clone | while | flops 87 | bytes 372 | solution.py:60
  56.8 0.6 gather_fusion.1
  57.5 0.6 gather_fusion.1
  58.2 0.6 gather_fusion.1
  63.2 0.6 gather_fusion.1
  63.9 0.6 gather_fusion.1
  64.6 0.6 gather_fusion.1
  65.3 0.6 gather_fusion.1
  66.0 0.6 gather_fusion.1
  66.8 5.9 %while.52 = (s32[]{:T(128)}, f32[1,8704]{1,0:T(1,128)S(1)}, s32[4,2]{0,1:T(2,128)S(1)}, f32[4,512]{1,0:T(4,128)S(1)}) while((s32[]{:T(128)}, f32[1,8704]{1,0:T(1,128)S(1)}, s32[4,2]{0,1:T(2,128)S(1)}, f32[4,512]{1,0:T(4,128)S(1)}) %tuple.112), condition=%wide.while_cond.1.clone, body=%wide.while_body.1.sunk.clone | while | flops 2 | bytes 8289 | solution.py:30
  67.5 0.8 constant_dynamic-slice_fusion.11
  68.9 0.8 constant_dynamic-slice_fusion.11
  70.4 0.8 constant_dynamic-slice_fusion.11
  71.9 0.8 constant_dynamic-slice_fusion.11
  72.7 29.2 %all-to-all-done = bf16[4,1,512,1024]{3,2,1,0:T(8,128)(2,1)} async-done(((bf16[4,1,512,1024]{3,2,1,0:T(8,128)(2,1)}), bf16[4,1,512,1024]{3,2,1,0:T(8,128)(2,1)}, u32[]{:S(2)}, u32[]{:S(2)}) %all-to-all-start) | async-done | bytes 4194336 | tf_op jit(solution)/shard_map/all_to_all | solution.py:83
  101.9 10.7 %fusion.12 = f32[2048,1024]{1,0:T(8,128)} fusion(bf16[2048,1024]{1,0:T(8,128)(2,1)} %bitcast.6, bf16[1,1024,1024]{2,1,0:T(8,128)(2,1)} %all-gather.5.cloned.1.call-done), kind=kOutput, calls=%fused_computation.38 | convolution fusion | flops 4294967296 | bytes 14680064 | tf_op jit(solution)/shard_map/erd,efd->erf/dot_general | solution.py:40
  112.6 14.5 %convolution_convert_fusion = bf16[2048,1024]{1,0:T(8,128)(2,1)} fusion(f32[2048,1024]{1,0:T(8,128)} %fusion.12, bf16[2048,1024]{1,0:T(8,128)(2,1)} %bitcast.6, bf16[1,1024,1024]{2,1,0:T(8,128)(2,1)} %all-gather.9.cloned.1.call-done, bf16[1,1024,1024]{2,1,0:T(8,128)(2,1)} %all-gather.7.cloned.1.call-done), kind=kOutput, calls=%fused_computation.29 | convolution fusion | flops 8604614656 | bytes 20971520 | tf_op jit(solution)/shard_map/erf,efd->erd/dot_general | solution.py:43
  127.1 2.9 %multiply_convert_fusion = bf16[4,1,512,1024]{3,2,1,0:T(8,128)(2,1)S(1)} fusion(bf16[4,1,512,1024]{3,2,0,1:T(8,128)(2,1)} %bitcast.87, f32[4,512]{1,0:T(4,128)S(1)} %get-tuple-element.152), kind=kLoop, calls=%fused_computation.26 | loop fusion | flops 6291456 | bytes 8396800 | tf_op jit(solution)/shard_map/convert_element_type | solution.py:18
  130.1 50.7 %all_to_all.10 = bf16[4,1,512,1024]{3,2,1,0:T(8,128)(2,1)} all-to-all(bf16[4,1,512,1024]{3,2,1,0:T(8,128)(2,1)S(1)} %multiply_convert_fusion), channel_id=1, replica_groups=mesh['ep'=4,'tp'=8] {'ep'}, dimensions={0} | all-to-all | bytes 8388608 | tf_op jit(solution)/shard_map/all_to_all | solution.py:101
  180.7 18.6 %scatter_custom_fusion = f32[513,1024]{1,0:T(8,128)S(1)} fusion(s32[2048]{0:T(1024)S(1)} %bitcast.90, bf16[2048,1024]{1,0:T(8,128)(2,1)} %bitcast.86, f32[]{:T(128)} %constant.92.clone.1), kind=kCustom, calls=%fused_computation.24 | custom fusion | flops 4194304 | bytes 6295556 | tf_op jit(solution)/shard_map/scatter-add | solution.py:105
  199.3 1.1 slice.37
  (150 shorter events, 11.3 us)
Async XLA Ops:
  6.5 30.1 %copy-start.1 = (bf16[512,1024]{1,0:T(8,128)(2,1)S(1)}, bf16[512,1024]{1,0:T(8,128)(2,1)}, u32[]{:S(2)}) copy-start(bf16[512,1024]{1,0:T(8,128)(2,1)} %param.11) | copy-start | bytes 3145732
  6.5 30.4 %copy-start.3 = (f32[1024]{0:T(1024)S(1)}, f32[1024]{0:T(1024)}, u32[]{:S(2)}) copy-start(f32[1024]{0:T(1024)} %param.12) | copy-start | bytes 12292
  6.5 95.4 %all-gather.5.cloned.1.call-start = ((), (), s32[]{:S(2)}) async-start(), calls=%async_computation.2 | async-start | bytes 2359296 | tf_op jit(solution)/shard_map/all_gather | solution.py:11
  7.3 105.4 %all-gather.9.cloned.1.call-start = ((), (), s32[]{:S(2)}) async-start(), calls=%async_computation.4 | async-start | bytes 2359296 | tf_op jit(solution)/shard_map/all_gather | solution.py:11
  50.9 5.8 %copy-start = (s32[1,8192]{1,0:T(1,128)S(1)}, s32[1,8192]{1,0:T(1,128)}, u32[]{:S(2)}) copy-start(s32[1,8192]{1,0:T(1,128)} %param.16) | copy-start | bytes 98308
  50.9 15.8 %copy-start.2 = (f32[1,8192]{1,0:T(1,128)S(1)}, f32[1,8192]{1,0:T(1,128)}, u32[]{:S(2)}) copy-start(f32[1,8192]{1,0:T(1,128)} %param.17) | copy-start | bytes 98308
  50.9 51.0 %all-to-all-start = ((bf16[4,1,512,1024]{3,2,1,0:T(8,128)(2,1)}), bf16[4,1,512,1024]{3,2,1,0:T(8,128)(2,1)}, u32[]{:S(2)}, u32[]{:S(2)}) async-start(bf16[4,1,512,1024]{3,2,1,0:T(8,128)(2,1)} %select_select_fusion), calls=%async_computation | async-start | bytes 8388608 | tf_op jit(solution)/shard_map/all_to_all | solution.py:83
  56.0 56.6 %all-gather.7.cloned.1.call-start = ((), (), s32[]{:S(2)}) async-start(), calls=%async_computation.3 | async-start | bytes 2359296 | tf_op jit(solution)/shard_map/all_gather | solution.py:11
Sparse Core Ops, SparseCore 0:
  8.9 31.9 all-gather.4
  42.5 28.5 all-gather.8
  72.7 28.4 all-gather.6
where the time goes:
time: 208 us; the launch traced here: 207 us
  blocking collectives  60.8 us (29%)
  local copies, waits for them, and re-layouts  43.5 us (21%)
  waiting for transfers between devices  31.3 us (15%)
  other arithmetic  26.9 us (13%)
  matrix products  25.2 us (12%)
  between operations  13.3 us (6%)
  starting transfers between devices  5.13 us (2%)
    all_to_all x1, blocking collectives, per_device(): lax.all_to_all(shortened(weighted), 'ep', split_axis=0, concat_axis=0, ti...  50.7 us
    all_to_all x1, waiting for transfers between devices, per_device(): lax.all_to_all(outgoing, 'ep', split_axis=0, concat_axis=0, tiled=True)  29.2 us
    scatter-add x1, other arithmetic, per_device(): jax.ops.segment_sum(returned.reshape(-1, feature_count), segment_ids, num...  18.6 us
    dot_general x1, matrix products, add_slice(): jnp.einsum('erf,efd->erd', hidden, down_piece, preferred_element_type=jnp...  14.5 us
    gather x32, local copies, waits for them, and re-layouts  14.3 us
    dot_general x1, matrix products, add_slice(): jnp.einsum('erd,efd->erf', inputs, gate_piece, preferred_element_type=jnp...  10.7 us
    all_gather x1, blocking collectives, per_device(): all_lists = lax.all_gather(chosen, 'ep', axis=0, tiled=True)  10.2 us
    gather x1, local copies, waits for them, and re-layouts, per_device(): outgoing = jnp.take(normed, safe_rows.reshape(-1), axis=0)  9.71 us
  transfers between devices with their start and end apart: 4, of which 1 were waited for; matrix products, arithmetic and copies ran while one was open for 28% of the time, Pallas kernels for 0%

commit v1 on v0

--- a/solution.py
+++ b/solution.py
@@ -1,6 +1,10 @@
+import functools
+
 import jax
 import jax.numpy as jnp
 from jax import lax
+from jax.experimental import pallas as pl
+from jax.experimental.pallas import tpu as pltpu
 from jax.sharding import PartitionSpec as P
 
 epsilon = 1e-06
@@ -45,7 +49,7 @@
     )
 
 
-def per_device(stream, norm_gain, gate_rows, up_rows, down_rows, chosen, affinity):
+def routed(stream, norm_gain, gate_rows, up_rows, down_rows, chosen, affinity):
     ep_count = lax.axis_size("ep")
     tp_count = lax.axis_size("tp")
     row_count, feature_count = stream.shape
@@ -108,6 +112,267 @@
     return summed[:row_count].astype(jnp.bfloat16)
 
 
+MESH = pl.DeviceIdType.MESH
+LANES = 128
+
+
+def dense_kernel(
+    chips,
+    stream_ref, gain_ref, gate_ref, up_ref, down_ref, chosen_ref, weight_ref,
+    out_ref,
+    arrived, normed, full, scale, hidden, far, near_x, near_y, held_x, held_y, own,
+    part_a, part_b, back_x, back_y,
+    local_sem, give_sem, pass_sem, take_sem,
+    token_send, token_pass, token_take, sum_send, sum_take,
+):
+    ep = lax.axis_index("ep")
+    tp = lax.axis_index("tp")
+    rows, width = stream_ref.shape
+    half = rows // 2
+    units = gate_ref.shape[0]
+    chip = tp // 2
+    core = lax.rem(tp, 2)
+    to_x = (jnp.bitwise_xor(ep, 1), tp)
+    to_y = (jnp.bitwise_xor(ep, 2), tp)
+    sibling = (ep, chip * 2 + 1 - core)
+    others = [(ep, lax.rem(chip + k, chips) * 2 + core) for k in range(1, chips)]
+    front = pl.ds(0, half)
+    rear = pl.ds(half, half)
+    mats = (gate_ref, up_ref, down_ref)
+
+    barrier = pltpu.get_barrier_semaphore()
+    peers = [to_x, to_y, sibling] + others
+    for peer in peers:
+        pl.semaphore_signal(barrier, inc=1, device_id=peer, device_id_type=MESH)
+    pl.semaphore_wait(barrier, len(peers))
+
+    def remote(source, target, sent, landed, peer):
+        return pltpu.make_async_remote_copy(
+            src_ref=source, dst_ref=target, send_sem=sent, recv_sem=landed,
+            device_id=peer, device_id_type=MESH,
+        )
+
+    sends = []
+
+    def launch(*spec):
+        copy = remote(*spec)
+        copy.start()
+        sends.append(copy)
+
+    def landed(target, sem, peer):
+        remote(target, target, sem, sem, peer).wait_recv()
+
+    def token(peer, slot, part, index):
+        launch(stream_ref.at[part], arrived.at[slot - 1, part], token_send.at[index],
+               token_take.at[slot, 0 if part is front else 1], peer)
+
+    def slot_rows(source):
+        return pl.ds(pl.multiple_of(source * units, units), units)
+
+    token(to_x, 1, front, 0)
+    token(to_y, 2, rear, 1)
+    for m in range(3):
+        for k in range(1, chips):
+            launch(mats[m], full.at[m, slot_rows(tp)], give_sem.at[m, k],
+                   take_sem.at[m, tp], others[k - 1])
+    token(to_x, 1, rear, 2)
+    token(to_y, 2, front, 3)
+    for m in range(3):
+        launch(mats[m], full.at[m, slot_rows(tp)], give_sem.at[m, 0],
+               take_sem.at[m, tp], sibling)
+    kept = []
+    for m in range(3):
+        copy = pltpu.make_async_copy(mats[m], full.at[m, slot_rows(tp)], local_sem.at[m])
+        copy.start()
+        kept.append(copy)
+
+    def normalize_block(load, slot):
+        def step(i, carry):
+            at = pl.ds(pl.multiple_of(i * 64, 64), 64)
+            values = load(at).astype(jnp.float32)
+            inverse = lax.rsqrt(jnp.mean(values * values, axis=-1, keepdims=True) + epsilon)
+            normed[slot, at, :] = (values * inverse * gain_ref[...]).astype(jnp.bfloat16)
+            return carry
+
+        lax.fori_loop(0, rows // 64, step, 0)
+
+    normalize_block(lambda at: stream_ref[at, :], 0)
+
+    tp_count = 2 * chips
+    window = 8 * ((rows // LANES + 1 + 7) // 8)
+    list_rows = chosen_ref.shape[0]
+    for slot in range(4):
+        first = (jnp.bitwise_xor(ep, slot) * tp_count + tp) * rows
+        before = (chosen_ref[:, LANES - 1:LANES] < first).astype(jnp.int32)
+        start = jnp.minimum(jnp.sum(before), list_rows - window)
+        names = chosen_ref[pl.ds(start, window), :]
+        values = weight_ref[pl.ds(start, window), :]
+        tokens = first + lax.broadcasted_iota(jnp.int32, (rows, LANES), 0)
+        total = jnp.zeros((rows, LANES), jnp.float32)
+        for r in range(window):
+            total += jnp.where(names[r:r + 1, :] == tokens, values[r:r + 1, :], 0.0)
+        scale[slot] = jnp.sum(total, axis=1, keepdims=True)
+
+    landed(arrived.at[0, front], token_take.at[1, 0], to_x)
+    launch(arrived.at[0, front], arrived.at[2, front], token_pass.at[0],
+           token_take.at[3, 0], to_y)
+    landed(arrived.at[1, rear], token_take.at[2, 1], to_y)
+    launch(arrived.at[1, rear], arrived.at[2, rear], token_pass.at[1],
+           token_take.at[3, 1], to_x)
+
+    def hand_on(m, k):
+        source = lax.rem(chip + chips - k, chips) * 2 + core
+        place = full.at[m, slot_rows(source)]
+        landed(place, take_sem.at[m, source], others[k - 1])
+        launch(place, place, pass_sem.at[m, k], take_sem.at[m, source], sibling)
+
+    for m in range(3):
+        for k in range(1, chips):
+            hand_on(m, k)
+
+    landed(arrived.at[0, rear], token_take.at[1, 1], to_x)
+    normalize_block(lambda at: arrived[0, at, :], 1)
+    landed(arrived.at[1, front], token_take.at[2, 0], to_y)
+    normalize_block(lambda at: arrived[1, at, :], 2)
+    landed(arrived.at[2, front], token_take.at[3, 0], to_y)
+    landed(arrived.at[2, rear], token_take.at[3, 1], to_x)
+    normalize_block(lambda at: arrived[2, at, :], 3)
+
+    for copy in kept:
+        copy.wait()
+    for m in range(3):
+        landed(full.at[m, slot_rows(sibling[1])], take_sem.at[m, sibling[1]], sibling)
+        for k in range(1, chips):
+            source = lax.rem(chip + chips - k, chips) * 2 + 1 - core
+            landed(full.at[m, slot_rows(source)], take_sem.at[m, source], sibling)
+
+    tile = min(256, width)
+
+    def expert(slot, keep):
+        def rise(i, carry):
+            at = pl.ds(pl.multiple_of(i * tile, tile), tile)
+            inputs = normed[slot]
+            dims = (((1,), (1,)), ((), ()))
+            gate = lax.dot_general(inputs, full[0, at, :], dims,
+                                   preferred_element_type=jnp.float32)
+            up = lax.dot_general(inputs, full[1, at, :], dims,
+                                 preferred_element_type=jnp.float32)
+            hidden[:, at] = (gate / (1.0 + jnp.exp(-gate)) * up).astype(jnp.bfloat16)
+            return carry
+
+        lax.fori_loop(0, full.shape[1] // tile, rise, 0)
+
+        def fall(i, carry):
+            at = pl.ds(pl.multiple_of(i * tile, tile), tile)
+            result = jnp.dot(hidden[...], full[2, :, at], preferred_element_type=jnp.float32)
+            keep(at, result.astype(jnp.bfloat16).astype(jnp.float32) * scale[slot])
+            return carry
+
+        lax.fori_loop(0, width // tile, fall, 0)
+
+    def keep_far(at, value):
+        far[:, at] = value.astype(jnp.bfloat16)
+
+    def keep_x(at, value):
+        near_x[0:half, at] = value[:half].astype(jnp.bfloat16)
+        held_x[:, at] = value[half:]
+
+    def keep_y(at, value):
+        near_y[half:rows, at] = value[half:].astype(jnp.bfloat16)
+        held_y[:, at] = value[:half]
+
+    def keep_own(at, value):
+        own[:, at] = value
+
+    expert(3, keep_far)
+    launch(far.at[front], part_a, sum_send.at[0], sum_take.at[0], to_x)
+    launch(far.at[rear], part_b, sum_send.at[1], sum_take.at[1], to_y)
+    expert(1, keep_x)
+    launch(near_x.at[front], back_x.at[front], sum_send.at[2], sum_take.at[2], to_x)
+    expert(2, keep_y)
+    launch(near_y.at[rear], back_y.at[rear], sum_send.at[3], sum_take.at[3], to_y)
+    expert(0, keep_own)
+    landed(part_a, sum_take.at[0], to_x)
+    near_y[0:half, :] = (held_y[...] + part_a[...].astype(jnp.float32)).astype(jnp.bfloat16)
+    launch(near_y.at[front], back_y.at[front], sum_send.at[4], sum_take.at[4], to_y)
+    landed(part_b, sum_take.at[1], to_y)
+    near_x[half:rows, :] = (held_x[...] + part_b[...].astype(jnp.float32)).astype(jnp.bfloat16)
+    launch(near_x.at[rear], back_x.at[rear], sum_send.at[5], sum_take.at[5], to_x)
+    landed(back_x.at[front], sum_take.at[2], to_x)
+    landed(back_y.at[rear], sum_take.at[3], to_y)
+    landed(back_y.at[front], sum_take.at[4], to_y)
+    out_ref[0:half, :] = (
+        own[0:half, :] + back_x[0:half, :].astype(jnp.float32)
+        + back_y[0:half, :].astype(jnp.float32)
+    ).astype(jnp.bfloat16)
+    landed(back_x.at[rear], sum_take.at[5], to_x)
+    out_ref[half:rows, :] = (
+        own[half:rows, :] + back_x[half:rows, :].astype(jnp.float32)
+        + back_y[half:rows, :].astype(jnp.float32)
+    ).astype(jnp.bfloat16)
+    for copy in sends:
+        copy.wait_send()
+
+
+def dense(stream, norm_gain, gate_rows, up_rows, down_rows, chosen, affinity):
+    tp_count = lax.axis_size("tp")
+    rows, width = stream.shape
+    half = rows // 2
+    units = gate_rows.shape[1]
+    hidden_count = units * tp_count
+    chips = tp_count // 2
+    vmem = pl.BlockSpec(memory_space=pltpu.VMEM)
+    low, wide = jnp.bfloat16, jnp.float32
+    dma = pltpu.SemaphoreType.DMA
+    return pl.pallas_call(
+        functools.partial(dense_kernel, chips),
+        out_shape=jax.ShapeDtypeStruct((rows, width), low),
+        in_specs=[vmem] * 7,
+        out_specs=vmem,
+        scratch_shapes=[
+            pltpu.VMEM((3, rows, width), low),
+            pltpu.VMEM((4, rows, width), low),
+            pltpu.VMEM((3, hidden_count, width), low),
+            pltpu.VMEM((4, rows, 1), wide),
+            pltpu.VMEM((rows, hidden_count), low),
+            pltpu.VMEM((rows, width), low),
+            pltpu.VMEM((rows, width), low),
+            pltpu.VMEM((rows, width), low),
+            pltpu.VMEM((half, width), wide),
+            pltpu.VMEM((half, width), wide),
+            pltpu.VMEM((rows, width), wide),
+            pltpu.VMEM((half, width), low),
+            pltpu.VMEM((half, width), low),
+            pltpu.VMEM((rows, width), low),
+            pltpu.VMEM((rows, width), low),
+            dma((3,)), dma((3, chips)), dma((3, chips)), dma((3, tp_count)),
+            dma((4,)), dma((2,)), dma((4, 2)), dma((6,)), dma((6,)),
+        ],
+        compiler_params=pltpu.CompilerParams(
+            collective_id=0, has_side_effects=True, vmem_limit_bytes=60 * 1024 * 1024
+        ),
+    )(
+        stream,
+        norm_gain.reshape(1, width),
+        gate_rows[0],
+        up_rows[0],
+        down_rows[0],
+        chosen.reshape(-1, LANES),
+        affinity.reshape(-1, LANES),
+    )
+
+
+def per_device(stream, norm_gain, gate_rows, up_rows, down_rows, chosen, affinity):
+    ep_count = lax.axis_size("ep")
+    tp_count = lax.axis_size("tp")
+    row_count = stream.shape[0]
+    local_experts = chosen.shape[0]
+    slot_count = 4 * row_count // (local_experts * ep_count)
+    if ep_count == 4 and local_experts == 1 and slot_count >= row_count and tp_count % 2 == 0:
+        return dense(stream, norm_gain, gate_rows, up_rows, down_rows, chosen, affinity)
+    return routed(stream, norm_gain, gate_rows, up_rows, down_rows, chosen, affinity)
+
+
 def solution(mesh):
     return jax.shard_map(
         per_device,

time: 208 us -> 120 us (0.58)
  the two profiles are of different devices: /device:TPU:0 before, /device:TPU:26 now
where the time goes in v1:
time: 120 us
  Pallas kernels  118 us (98%)
  local copies, waits for them, and re-layouts  2.26 us (2%)
    pallas_call x1, Pallas kernels, dense(): pl.pallas_call(functools.partial(dense_kernel, chips), out_shape=jax.Shap...  118 us

profile of v1, /device:TPU:26, one launch (start us, length us, event | category | flops | bytes accessed | tf_op | source)
XLA Modules:
  0.0 120.1 jit_solution(8536552574226460411)
XLA Ops:
  0.0 117.9 %shard_map.73 = bf16[512,1024]{1,0:T(8,128)(2,1)} custom-call(bf16[512,1024]{1,0:T(8,128)(2,1)} %stream_ref.1, f32[1,1024]{1,0:T(1,128)} %bitcast.11, bf16[128,1024]{1,0:T(8,128)(2,1)} %bitcast.6, bf16[128,1024]{1,0:T(8,128)(2,1)} %bitcast.7, bf16[128,1024]{1,0:T(8,128)(2,1)} %bitcast.8, s32[64,128]{1,0:T(8,128)} %bitcast.9, f32[64,128]{1,0:T(8,128)} %bitcast.10), custom_call_target="tpu_custom_call" | custom-call | tf_op jit(solution)/shard_map/pallas_call | solution.py:327
  117.9 2.3 %copy.9 = bf16[512,1024]{1,0:T(8,128)(2,1)} copy(bf16[512,1024]{1,0:T(8,128)(2,1)} %shard_map.73) | data formatting | bytes 2097152

commit v2 on v1

--- a/solution.py
+++ b/solution.py
@@ -122,7 +122,7 @@
     out_ref,
     arrived, normed, full, scale, hidden, far, near_x, near_y, held_x, held_y, own,
     part_a, part_b, back_x, back_y,
-    local_sem, give_sem, pass_sem, take_sem,
+    local_sem, give_sem, pass_sem, side_sem, take_sem,
     token_send, token_pass, token_take, sum_send, sum_take,
 ):
     ep = lax.axis_index("ep")
@@ -135,16 +135,23 @@
     to_x = (jnp.bitwise_xor(ep, 1), tp)
     to_y = (jnp.bitwise_xor(ep, 2), tp)
     sibling = (ep, chip * 2 + 1 - core)
-    others = [(ep, lax.rem(chip + k, chips) * 2 + core) for k in range(1, chips)]
+    has_left = chip > 0
+    has_right = chip < chips - 1
+    left = (ep, tp - 2)
+    right = (ep, tp + 2)
     front = pl.ds(0, half)
     rear = pl.ds(half, half)
     mats = (gate_ref, up_ref, down_ref)
 
     barrier = pltpu.get_barrier_semaphore()
-    peers = [to_x, to_y, sibling] + others
-    for peer in peers:
-        pl.semaphore_signal(barrier, inc=1, device_id=peer, device_id_type=MESH)
-    pl.semaphore_wait(barrier, len(peers))
+    peers = ((True, to_x), (True, to_y), (True, sibling), (has_left, left), (has_right, right))
+    for there, peer in peers:
+        @pl.when(there)
+        def _():
+            pl.semaphore_signal(barrier, inc=1, device_id=peer, device_id_type=MESH)
+    pl.semaphore_wait(
+        barrier, 3 + has_left.astype(jnp.int32) + has_right.astype(jnp.int32)
+    )
 
     def remote(source, target, sent, landed, peer):
         return pltpu.make_async_remote_copy(
@@ -154,10 +161,11 @@
 
     sends = []
 
-    def launch(*spec):
-        copy = remote(*spec)
-        copy.start()
-        sends.append(copy)
+    def launch(*spec, there=True):
+        @pl.when(there)
+        def _():
+            remote(*spec).start()
+        sends.append((there, spec))
 
     def landed(target, sem, peer):
         remote(target, target, sem, sem, peer).wait_recv()
@@ -171,15 +179,17 @@
 
     token(to_x, 1, front, 0)
     token(to_y, 2, rear, 1)
-    for m in range(3):
-        for k in range(1, chips):
-            launch(mats[m], full.at[m, slot_rows(tp)], give_sem.at[m, k],
-                   take_sem.at[m, tp], others[k - 1])
+    def give(m):
+        place = full.at[m, slot_rows(tp)]
+        landing = take_sem.at[m, tp]
+        launch(mats[m], place, give_sem.at[m, 0], landing, left, there=has_left)
+        launch(mats[m], place, give_sem.at[m, 1], landing, right, there=has_right)
+        launch(mats[m], place, give_sem.at[m, 2], landing, sibling)
+
+    give(0)
+    give(1)
     token(to_x, 1, rear, 2)
     token(to_y, 2, front, 3)
-    for m in range(3):
-        launch(mats[m], full.at[m, slot_rows(tp)], give_sem.at[m, 0],
-               take_sem.at[m, tp], sibling)
     kept = []
     for m in range(3):
         copy = pltpu.make_async_copy(mats[m], full.at[m, slot_rows(tp)], local_sem.at[m])
@@ -213,42 +223,44 @@
             total += jnp.where(names[r:r + 1, :] == tokens, values[r:r + 1, :], 0.0)
         scale[slot] = jnp.sum(total, axis=1, keepdims=True)
 
-    landed(arrived.at[0, front], token_take.at[1, 0], to_x)
-    launch(arrived.at[0, front], arrived.at[2, front], token_pass.at[0],
-           token_take.at[3, 0], to_y)
-    landed(arrived.at[1, rear], token_take.at[2, 1], to_y)
-    launch(arrived.at[1, rear], arrived.at[2, rear], token_pass.at[1],
-           token_take.at[3, 1], to_x)
-
     def hand_on(m, k):
-        source = lax.rem(chip + chips - k, chips) * 2 + core
-        place = full.at[m, slot_rows(source)]
-        landed(place, take_sem.at[m, source], others[k - 1])
-        launch(place, place, pass_sem.at[m, k], take_sem.at[m, source], sibling)
-
-    for m in range(3):
-        for k in range(1, chips):
-            hand_on(m, k)
-
-    landed(arrived.at[0, rear], token_take.at[1, 1], to_x)
-    normalize_block(lambda at: arrived[0, at, :], 1)
-    landed(arrived.at[1, front], token_take.at[2, 0], to_y)
-    normalize_block(lambda at: arrived[1, at, :], 2)
-    landed(arrived.at[2, front], token_take.at[3, 0], to_y)
-    landed(arrived.at[2, rear], token_take.at[3, 1], to_x)
-    normalize_block(lambda at: arrived[2, at, :], 3)
-
-    for copy in kept:
-        copy.wait()
-    for m in range(3):
-        landed(full.at[m, slot_rows(sibling[1])], take_sem.at[m, sibling[1]], sibling)
-        for k in range(1, chips):
-            source = lax.rem(chip + chips - k, chips) * 2 + 1 - core
+        for side, there, origin, source_chip, onward, more in (
+            (0, chip >= k, left, chip - k, right, has_right),
+            (1, chip + k < chips, right, chip + k, left, has_left),
+        ):
+            source = source_chip * 2 + core
+            place = full.at[m, slot_rows(source)]
+            landing = take_sem.at[m, source]
+
+            @pl.when(there)
+            def _():
+                landed(place, landing, origin)
+
+            launch(place, place, pass_sem.at[m, side, k], landing, onward,
+                   there=jnp.logical_and(there, more))
+            launch(place, place, side_sem.at[m, side, k], landing, sibling, there=there)
+
+    def from_sibling(m):
+        for j in range(chips):
+            source = j * 2 + 1 - core
             landed(full.at[m, slot_rows(source)], take_sem.at[m, source], sibling)
 
+    for k in range(1, chips):
+        if k == 2 or chips == 2:
+            give(2)
+        hand_on(0, k)
+        hand_on(1, k)
+        if k == 1:
+            landed(arrived.at[0, front], token_take.at[1, 0], to_x)
+            launch(arrived.at[0, front], arrived.at[2, front], token_pass.at[0],
+                   token_take.at[3, 0], to_y)
+            landed(arrived.at[1, rear], token_take.at[2, 1], to_y)
+            launch(arrived.at[1, rear], arrived.at[2, rear], token_pass.at[1],
+                   token_take.at[3, 1], to_x)
+
     tile = min(256, width)
 
-    def expert(slot, keep):
+    def rise_block(slot):
         def rise(i, carry):
             at = pl.ds(pl.multiple_of(i * tile, tile), tile)
             inputs = normed[slot]
@@ -257,18 +269,41 @@
                                    preferred_element_type=jnp.float32)
             up = lax.dot_general(inputs, full[1, at, :], dims,
                                  preferred_element_type=jnp.float32)
-            hidden[:, at] = (gate / (1.0 + jnp.exp(-gate)) * up).astype(jnp.bfloat16)
+            hidden[slot, :, at] = (gate / (1.0 + jnp.exp(-gate)) * up).astype(jnp.bfloat16)
             return carry
 
         lax.fori_loop(0, full.shape[1] // tile, rise, 0)
 
+    def fall_block(slot, keep):
         def fall(i, carry):
             at = pl.ds(pl.multiple_of(i * tile, tile), tile)
-            result = jnp.dot(hidden[...], full[2, :, at], preferred_element_type=jnp.float32)
+            result = jnp.dot(hidden[slot], full[2, :, at], preferred_element_type=jnp.float32)
             keep(at, result.astype(jnp.bfloat16).astype(jnp.float32) * scale[slot])
             return carry
 
         lax.fori_loop(0, width // tile, fall, 0)
+
+    for copy in kept:
+        copy.wait()
+    from_sibling(0)
+    from_sibling(1)
+    later = list(range(1, chips))
+    for slot in range(4):
+        if slot == 1:
+            landed(arrived.at[0, rear], token_take.at[1, 1], to_x)
+            normalize_block(lambda at: arrived[0, at, :], 1)
+        elif slot == 2:
+            landed(arrived.at[1, front], token_take.at[2, 0], to_y)
+            normalize_block(lambda at: arrived[1, at, :], 2)
+        elif slot == 3:
+            landed(arrived.at[2, front], token_take.at[3, 0], to_y)
+            landed(arrived.at[2, rear], token_take.at[3, 1], to_x)
+            normalize_block(lambda at: arrived[2, at, :], 3)
+        rise_block(slot)
+        for k in later[:1] if slot < 3 else later:
+            hand_on(2, k)
+        later = later[1:] if slot < 3 else []
+    from_sibling(2)
 
     def keep_far(at, value):
         far[:, at] = value.astype(jnp.bfloat16)
@@ -284,14 +319,14 @@
     def keep_own(at, value):
         own[:, at] = value
 
-    expert(3, keep_far)
+    fall_block(3, keep_far)
     launch(far.at[front], part_a, sum_send.at[0], sum_take.at[0], to_x)
     launch(far.at[rear], part_b, sum_send.at[1], sum_take.at[1], to_y)
-    expert(1, keep_x)
+    fall_block(1, keep_x)
     launch(near_x.at[front], back_x.at[front], sum_send.at[2], sum_take.at[2], to_x)
-    expert(2, keep_y)
+    fall_block(2, keep_y)
     launch(near_y.at[rear], back_y.at[rear], sum_send.at[3], sum_take.at[3], to_y)
-    expert(0, keep_own)
+    fall_block(0, keep_own)
     landed(part_a, sum_take.at[0], to_x)
     near_y[0:half, :] = (held_y[...] + part_a[...].astype(jnp.float32)).astype(jnp.bfloat16)
     launch(near_y.at[front], back_y.at[front], sum_send.at[4], sum_take.at[4], to_y)
@@ -310,8 +345,10 @@
         own[half:rows, :] + back_x[half:rows, :].astype(jnp.float32)
         + back_y[half:rows, :].astype(jnp.float32)
     ).astype(jnp.bfloat16)
-    for copy in sends:
-        copy.wait_send()
+    for there, spec in sends:
+        @pl.when(there)
+        def _():
+            remote(*spec).wait_send()
 
 
 def dense(stream, norm_gain, gate_rows, up_rows, down_rows, chosen, affinity):
@@ -334,7 +371,7 @@
             pltpu.VMEM((4, rows, width), low),
             pltpu.VMEM((3, hidden_count, width), low),
             pltpu.VMEM((4, rows, 1), wide),
-            pltpu.VMEM((rows, hidden_count), low),
+            pltpu.VMEM((4, rows, hidden_count), low),
             pltpu.VMEM((rows, width), low),
             pltpu.VMEM((rows, width), low),
             pltpu.VMEM((rows, width), low),
@@ -345,7 +382,7 @@
             pltpu.VMEM((half, width), low),
             pltpu.VMEM((rows, width), low),
             pltpu.VMEM((rows, width), low),
-            dma((3,)), dma((3, chips)), dma((3, chips)), dma((3, tp_count)),
+            dma((3,)), dma((3, 3)), dma((3, 2, chips)), dma((3, 2, chips)), dma((3, tp_count)),
             dma((4,)), dma((2,)), dma((4, 2)), dma((6,)), dma((6,)),
         ],
         compiler_params=pltpu.CompilerParams(

time: 120 us -> 105 us (0.88)
  the two profiles are of different devices: /device:TPU:26 before, /device:TPU:0 now
where the time goes in v2:
time: 105 us
  Pallas kernels  103 us (98%)
  local copies, waits for them, and re-layouts  2.26 us (2%)
    pallas_call x1, Pallas kernels, dense(): pl.pallas_call(functools.partial(dense_kernel, chips), out_shape=jax.Shap...  103 us
    unnamed x1, local copies, waits for them, and re-layouts  2.26 us

profile of v2, /device:TPU:0, one launch (start us, length us, event | category | flops | bytes accessed | tf_op | source)
XLA Modules:
  0.0 104.8 jit_solution(12862968119902020219)
XLA Ops:
  0.0 102.5 %shard_map.73 = bf16[512,1024]{1,0:T(8,128)(2,1)} custom-call(bf16[512,1024]{1,0:T(8,128)(2,1)} %stream_ref.1, f32[1,1024]{1,0:T(1,128)} %bitcast.11, bf16[128,1024]{1,0:T(8,128)(2,1)} %bitcast.6, bf16[128,1024]{1,0:T(8,128)(2,1)} %bitcast.7, bf16[128,1024]{1,0:T(8,128)(2,1)} %bitcast.8, s32[64,128]{1,0:T(8,128)} %bitcast.9, f32[64,128]{1,0:T(8,128)} %bitcast.10), custom_call_target="tpu_custom_call" | custom-call | tf_op jit(solution)/shard_map/pallas_call | solution.py:364
  102.5 2.3 %copy.9 = bf16[512,1024]{1,0:T(8,128)(2,1)} copy(bf16[512,1024]{1,0:T(8,128)(2,1)} %shard_map.73) | data formatting | bytes 2097152
